TPU v7x, 32 devices: a whole 2x2x4 slice. The times are simulated.
32 devices in a mesh: ep: 8 (over z, core), tp: 4 (over y, x).
Axes of the slice: x: 2, y: 2, z: 4, core: 2. Of those that a mesh axis runs over, the one named last changes fastest.
Arguments:
- tokens: bfloat16 [256, 4096], P('ep'), may hold values from -6 to 6
- recur_state: float32 [256, 4096], P('ep', 'tp'), may hold values from -6 to 6
- conv_state: bfloat16 [256, 3, 4096], P('ep', None, 'tp'), may hold values from -6 to 6
- mix_gain: float32 [4096], replicated, may hold values from 0.1 to 1.9
- in_weight: bfloat16 [4096, 4096], P('ep', 'tp'), may hold values from -0.09375 to 0.09375
- gate_weight: bfloat16 [4096, 4096], P('ep', 'tp'), may hold values from -0.09375 to 0.09375
- conv_taps: float32 [4, 4096], P(None, 'tp'), may hold values from -3 to 3
- recur_gate_blocks: bfloat16 [64, 64, 64], P('tp'), may hold values from -0.75 to 0.75
- input_gate_blocks: bfloat16 [64, 64, 64], P('tp'), may hold values from -0.75 to 0.75
- decay_rate: float32 [4096], P('tp'), may hold values from 0.01 to 0.4
- out_weight: bfloat16 [4096, 4096], P('tp', 'ep'), may hold values from -0.09375 to 0.09375
- ffn_gain: float32 [4096], replicated, may hold values from 0.1 to 1.9
- router_weight: bfloat16 [4096, 8], replicated, may hold values from -0.09375 to 0.09375
- routes: int32 [256, 2], P('ep'), may hold values from 0 to 7, as said below
- expert_gate: bfloat16 [8, 4096, 2048], P('ep', None, 'tp'), may hold values from -0.09375 to 0.09375
- expert_up: bfloat16 [8, 4096, 2048], P('ep', None, 'tp'), may hold values from -0.09375 to 0.09375
- expert_down: bfloat16 [8, 2048, 4096], P('ep', 'tp'), may hold values from -0.125 to 0.125
- dense_gate: bfloat16 [4096, 2048], P('ep', 'tp'), may hold values from -0.09375 to 0.09375
- dense_up: bfloat16 [4096, 2048], P('ep', 'tp'), may hold values from -0.09375 to 0.09375
- dense_down: bfloat16 [2048, 4096], P('tp', 'ep'), may hold values from -0.125 to 0.125
- branch_gate: bfloat16 [4096], replicated, may hold values from -0.09375 to 0.09375
Outputs:
- layer_out: bfloat16 [256, 4096], P('ep')
- new_state: float32 [256, 4096], P('ep', 'tp')
- new_conv_state: bfloat16 [256, 3, 4096], P('ep', None, 'tp')
Inputs may be any that keep to these rules, and one draw needn't show every extreme that they name: `routes`: A row names two different experts of one group: both have the same e // 4. In the rows of one index of ep no expert is named more than 16 times, and in every draw some expert is named exactly 16 times by the rows of every index of ep.
All inputs are finite; a program needn't handle non-finite values.
Results may differ from a plain program's by a relative error of at most 0.023.
Values may be sent and summed in bfloat16 or wider, within the bound.
A program may use at most 64 MiB of HBM per device.

v0:
```python
import jax
import jax.numpy as jnp
from jax import lax
from jax.sharding import PartitionSpec as P

TOP_K = 2
epsilon = 1e-06
decay_scale = 8.0


def rms_scale(rows, gain):
    values = rows.astype(jnp.float32)
    inverse = lax.rsqrt(jnp.mean(values * values, axis=-1, keepdims=True) + epsilon)
    return (values * inverse * gain).astype(jnp.bfloat16)


def on_device(
    tokens,
    recur_state,
    conv_state,
    mix_gain,
    in_weight,
    gate_weight,
    conv_taps,
    recur_gate_blocks,
    input_gate_blocks,
    decay_rate,
    out_weight,
    ffn_gain,
    router_weight,
    routes,
    expert_gate,
    expert_up,
    expert_down,
    dense_gate,
    dense_up,
    dense_down,
    branch_gate,
):
    batch_rows, width = tokens.shape
    channels = in_weight.shape[1]
    normed = rms_scale(tokens, mix_gain)
    arrived = lax.all_to_all(normed, "ep", split_axis=1, concat_axis=0, tiled=True)
    joined = jnp.concatenate([in_weight, gate_weight], axis=1)
    summed = lax.psum_scatter(
        jnp.dot(arrived, joined, preferred_element_type=jnp.float32).astype(jnp.bfloat16),
        "ep",
        scatter_dimension=0,
        tiled=True,
    ).astype(jnp.float32)
    x_sum, gate_sum = (summed[:, :channels], summed[:, channels:])
    x_branch = x_sum.astype(jnp.bfloat16)
    gate_branch = gate_sum.astype(jnp.bfloat16)
    window = jnp.concatenate([conv_state, x_branch[:, None, :]], axis=1)
    conv_out = jnp.sum(window.astype(jnp.float32) * conv_taps[None], axis=1).astype(jnp.bfloat16)
    new_conv_state = window[:, 1:, :]
    blocks = conv_out.reshape(batch_rows, recur_gate_blocks.shape[0], recur_gate_blocks.shape[1])
    recur_gate = jax.nn.sigmoid(
        jnp.einsum(
            "bhi,hij->bhj", blocks, recur_gate_blocks, preferred_element_type=jnp.float32
        ).reshape(batch_rows, channels)
    )
    input_gate = jax.nn.sigmoid(
        jnp.einsum(
            "bhi,hij->bhj", blocks, input_gate_blocks, preferred_element_type=jnp.float32
        ).reshape(batch_rows, channels)
    )
    log_decay = -decay_scale * recur_gate * decay_rate
    new_state = jnp.exp(log_decay) * recur_state + jnp.sqrt(
        -jnp.expm1(2.0 * log_decay)
    ) * input_gate * conv_out.astype(jnp.float32)
    mixer_rows = (new_state * jax.nn.gelu(gate_branch.astype(jnp.float32))).astype(jnp.bfloat16)
    mixer_part = jnp.dot(
        mixer_rows,
        lax.all_gather(out_weight, "ep", axis=1, tiled=True),
        preferred_element_type=jnp.float32,
    )
    resid = (
        tokens.astype(jnp.float32)
        + lax.psum(mixer_part.astype(jnp.bfloat16), "tp").astype(jnp.float32)
    ).astype(jnp.bfloat16)
    normed_ffn = rms_scale(resid, ffn_gain)
    router_logits = jnp.dot(normed_ffn, router_weight, preferred_element_type=jnp.float32)
    experts = router_logits.shape[1]
    expert_ids = lax.broadcasted_iota(jnp.int32, (batch_rows, TOP_K, experts), 2)
    picked = jnp.sum(
        jnp.where(routes[:, :, None] == expert_ids, router_logits[:, None, :], 0.0), axis=2
    )
    route_weight = jax.nn.sigmoid(picked - picked[:, ::-1]).astype(jnp.bfloat16)
    capacity = 2 * batch_rows * TOP_K // experts
    flat_ids = routes.reshape(batch_rows * TOP_K)
    onehot = (
        flat_ids[:, None] == lax.broadcasted_iota(jnp.int32, (batch_rows * TOP_K, experts), 1)
    ).astype(jnp.int32)
    rank = jnp.sum((jnp.cumsum(onehot, axis=0) - onehot) * onehot, axis=1)
    slot_of = (flat_ids * capacity + rank).reshape(batch_rows, TOP_K)
    slot_rows = lax.broadcasted_iota(jnp.int32, (experts * capacity, batch_rows), 0)
    slot_cols = lax.broadcasted_iota(jnp.int32, (batch_rows, experts * capacity), 1)
    dispatch = jnp.zeros((experts * capacity, batch_rows), jnp.bfloat16)
    combine = jnp.zeros((batch_rows, experts * capacity), jnp.bfloat16)
    for pick in range(TOP_K):
        dispatch = dispatch + (slot_rows == slot_of[None, :, pick]).astype(jnp.bfloat16)
        combine = combine + jnp.where(
            slot_cols == slot_of[:, pick : pick + 1],
            route_weight[:, pick : pick + 1],
            jnp.zeros((), jnp.bfloat16),
        )
    outgoing = (
        jnp.dot(dispatch, normed_ffn, preferred_element_type=jnp.float32)
        .astype(jnp.bfloat16)
        .reshape(experts, capacity, width)
    )
    gate_local = expert_gate[0]
    up_local = expert_up[0]
    down_local = expert_down[0]
    arrived_rows = lax.all_to_all(outgoing, "ep", split_axis=0, concat_axis=0, tiled=True)
    sources, items, features = arrived_rows.shape
    rows = arrived_rows.reshape(sources * items, features)
    first = jnp.dot(rows, gate_local, preferred_element_type=jnp.float32)
    second = jnp.dot(rows, up_local, preferred_element_type=jnp.float32)
    act = (jax.nn.silu(first) * second).astype(jnp.bfloat16)
    partial_value = jnp.dot(act, down_local, preferred_element_type=jnp.float32)
    total = lax.psum(partial_value.astype(jnp.bfloat16), "tp")
    returned = lax.all_to_all(
        total.reshape(sources, items, total.shape[1]), "ep", split_axis=0, concat_axis=0, tiled=True
    )
    moe = jnp.dot(
        combine,
        returned.reshape(experts * capacity, returned.shape[2]),
        preferred_element_type=jnp.float32,
    )
    dense_arrived = lax.all_to_all(normed_ffn, "ep", split_axis=1, concat_axis=0, tiled=True)
    dense_joined = jnp.concatenate([dense_gate, dense_up], axis=1)
    dense_summed = lax.psum_scatter(
        jnp.dot(dense_arrived, dense_joined, preferred_element_type=jnp.float32).astype(
            jnp.bfloat16
        ),
        "ep",
        scatter_dimension=0,
        tiled=True,
    ).astype(jnp.float32)
    dense_first = dense_summed[:, : dense_gate.shape[1]]
    dense_second = dense_summed[:, dense_gate.shape[1] :]
    dense_act = (jax.nn.silu(dense_first) * dense_second).astype(jnp.bfloat16)
    dense_part = jnp.dot(
        dense_act,
        lax.all_gather(dense_down, "ep", axis=1, tiled=True),
        preferred_element_type=jnp.float32,
    )
    branch_weight = jax.nn.sigmoid(
        jnp.dot(normed_ffn, branch_gate, preferred_element_type=jnp.float32)
    )
    dense_sum = lax.psum(dense_part.astype(jnp.bfloat16), "tp").astype(jnp.float32)
    layer_out = (resid.astype(jnp.float32) + moe + branch_weight[:, None] * dense_sum).astype(
        jnp.bfloat16
    )
    return (layer_out, new_state, new_conv_state)


def solution(mesh):
    in_specs = (
        P("ep", None),
        P("ep", "tp"),
        P("ep", None, "tp"),
        P(),
        P("ep", "tp"),
        P("ep", "tp"),
        P(None, "tp"),
        P("tp", None, None),
        P("tp", None, None),
        P("tp"),
        P("tp", "ep"),
        P(),
        P(),
        P("ep", None),
        P("ep", None, "tp"),
        P("ep", None, "tp"),
        P("ep", "tp", None),
        P("ep", "tp"),
        P("ep", "tp"),
        P("tp", "ep"),
        P(),
    )
    out_specs = (P("ep", None), P("ep", "tp"), P("ep", None, "tp"))
    return jax.shard_map(
        on_device, mesh=mesh, in_specs=in_specs, out_specs=out_specs, check_vma=False
    )
```

profile of v0, /device:TPU:0, one launch (start us, length us, event | category | flops | bytes accessed | tf_op | source)
XLA Modules:
  0.0 396.9 jit_solution(11186199223250125864)
XLA Ops:
  7.2 1.1 fusion.33
  8.4 1.1 fusion.35
  9.5 16.0 %all_to_all.48 = bf16[32,8,512]{2,0,1:T(8,128)(2,1)S(1)} all-to-all(bf16[32,8,512]{2,0,1:T(8,128)(2,1)S(1)} %bitcast.77), channel_id=1, replica_groups=mesh['ep'=8,'tp'=4] {'ep'}, dimensions={1} | all-to-all | bytes 524288 | tf_op jit(solution)/shard_map/all_to_all | solution.py:43
  25.5 3.4 convolution_convert_fusion.4
  29.0 0.7 all-gather.3.cloned.1.call-update
  29.8 30.9 %reduce-scatter.3.cloned.1.call-done = bf16[32,2048]{1,0:T(8,128)(2,1)} async-done(((bf16[256,2048]{1,0:T(8,128)(2,1)}), bf16[32,2048]{1,0:T(8,128)(2,1)}) %reduce-scatter.3.cloned.1.call-update) | async-done | bytes 131088 | tf_op jit(solution)/shard_map/reduce_scatter | solution.py:45
  60.7 0.9 slice_bitcast_fusion
  61.9 0.2 fusion.17
  62.4 0.2 fusion.13
  63.1 79.5 %all-gather.3.cloned.1.call-done = bf16[1024,4096]{1,0:T(8,128)(2,1)} async-done(((bf16[1024,512]{1,0:T(8,128)(2,1)}), bf16[1024,4096]{1,0:T(8,128)(2,1)}) %all-gather.3.cloned.1.call-update) | async-done | bytes 8388624 | tf_op jit(solution)/shard_map/all_gather | solution.py:75
  142.5 5.6 %convolution_convert_fusion.3 = bf16[32,4096]{1,0:T(8,128)(2,1)} fusion(bf16[1024,4096]{1,0:T(8,128)(2,1)} %all-gather.3.cloned.1.call-done, f32[32,1024]{1,0:T(8,128)S(1)} %multiply_add_fusion, bf16[32,2048]{1,0:T(8,128)(2,1)S(1)} %copy-done.5), kind=kOutput, calls=%fused_computation.6 | convolution fusion | flops 268926976 | bytes 8847360 | tf_op jit(solution)/shard_map/dot_general | solution.py:73
  148.2 41.6 %all-reduce.4.cloned.1.call-done = bf16[32,4096]{1,0:T(8,128)(2,1)} async-done(((bf16[32,4096]{1,0:T(8,128)(2,1)}), bf16[32,4096]{1,0:T(8,128)(2,1)}) %all-reduce.4.cloned.1.call-update) | async-done | bytes 262160 | tf_op jit(solution)/shard_map/psum | solution.py:80
  189.9 1.1 fusion.37
  191.0 1.1 fusion.39
  192.1 14.1 %all_to_all.49 = bf16[32,8,512]{2,0,1:T(8,128)(2,1)S(1)} all-to-all(bf16[32,8,512]{2,0,1:T(8,128)(2,1)S(1)} %bitcast.78), channel_id=1, replica_groups=mesh['ep'=8,'tp'=4] {'ep'}, dimensions={1} | all-to-all | bytes 524288 | tf_op jit(solution)/shard_map/all_to_all | solution.py:132
  206.2 1.3 convolution_convert_fusion.5
  207.6 0.5 all-gather.5.cloned.1.call-update
  208.5 0.2 select_reduce_fusion
  208.9 1.4 convolution_convert_fusion.1
  210.3 3.6 all-to-all-start.1
  213.9 24.5 %reduce-scatter.5.cloned.1.call-done = bf16[32,1024]{1,0:T(8,128)(2,1)} async-done(((bf16[256,1024]{1,0:T(8,128)(2,1)}), bf16[32,1024]{1,0:T(8,128)(2,1)}) %reduce-scatter.5.cloned.1.call-update) | async-done | bytes 65552 | tf_op jit(solution)/shard_map/reduce_scatter | solution.py:134
  238.4 0.8 convert_element_type.109
  239.2 49.8 %all-gather.5.cloned.1.call-done = bf16[512,4096]{1,0:T(8,128)(2,1)} async-done(((bf16[512,512]{1,0:T(8,128)(2,1)}), bf16[512,4096]{1,0:T(8,128)(2,1)}) %all-gather.5.cloned.1.call-update) | async-done | bytes 4194320 | tf_op jit(solution)/shard_map/all_gather | solution.py:147
  289.0 3.7 convolution_convert_fusion.2
  292.7 2.9 fusion.5
  295.7 5.9 %convolution_convert_fusion = bf16[128,4096]{1,0:T(8,128)(2,1)} fusion(bf16[1,512,4096]{2,1,0:T(8,128)(2,1)} %param.37, bf16[128,4096]{1,0:T(8,128)(2,1)S(1)} %bitcast.72, bf16[1,4096,512]{2,1,0:T(8,128)(2,1)} %param.36, f32[128,512]{1,0:T(8,128)S(1)} %fusion.5), kind=kOutput, calls=%fused_computation | convolution fusion | flops 1074659328 | bytes 10747904 | tf_op jit(solution)/shard_map/dot_general | solution.py:122
  301.6 55.4 %all-reduce.6.cloned.1.call-done = (bf16[8,16,4096]{2,1,0:T(8,128)(2,1)}, bf16[32,4096]{1,0:T(8,128)(2,1)}) async-done(((bf16[8,16,4096]{2,1,0:T(8,128)(2,1)}, bf16[32,4096]{1,0:T(8,128)(2,1)}), (bf16[8,16,4096]{2,1,0:T(8,128)(2,1)}, bf16[32,4096]{1,0:T(8,128)(2,1)})) %all-reduce.6.cloned.1.call-update) | async-done | bytes 1310736 | tf_op jit(solution)/shard_map/psum | solution.py:123
  356.9 4.6 %all-to-all-start.2 = ((bf16[8,16,4096]{2,1,0:T(8,128)(2,1)}), bf16[8,16,4096]{2,1,0:T(8,128)(2,1)S(1)}, u32[]{:S(2)}, u32[]{:S(2)}) async-start(bf16[8,16,4096]{2,1,0:T(8,128)(2,1)} %get-tuple-element.3), calls=%async_computation.3 | async-start | bytes 2097152 | tf_op jit(solution)/shard_map/all_to_all | solution.py:124
  361.5 0.7 fusion.45
  362.5 0.2 fusion.27
  362.7 25.4 %all-to-all-done.2 = bf16[8,16,4096]{2,1,0:T(8,128)(2,1)S(1)} async-done(((bf16[8,16,4096]{2,1,0:T(8,128)(2,1)}), bf16[8,16,4096]{2,1,0:T(8,128)(2,1)S(1)}, u32[]{:S(2)}, u32[]{:S(2)}) %all-to-all-start.2) | async-done | bytes 1048608 | tf_op jit(solution)/shard_map/all_to_all | solution.py:124
  388.1 2.0 fusion.1
  (69 shorter events, 2.2 us)
Async XLA Ops:
  7.2 54.7 %copy-start = (bf16[16,64,64]{2,1,0:T(8,128)(2,1)S(1)}, bf16[16,64,64]{2,1,0:T(8,128)(2,1)}, u32[]{:S(2)}) copy-start(bf16[16,64,64]{2,1,0:T(8,128)(2,1)} %param.28) | copy-start | bytes 393220
  7.2 53.5 %reduce-scatter.3.cloned.1.call-start = ((), (), s32[]{:S(2)}) async-start(), calls=%async_computation.6 | async-start | bytes 1179648 | tf_op jit(solution)/shard_map/reduce_scatter | solution.py:45
  8.4 21.4 %copy-start.12 = (f32[1024]{0:T(1024)S(1)}, f32[1024]{0:T(1024)}, u32[]{:S(2)}) copy-start(f32[1024]{0:T(1024)} %param.30) | copy-start | bytes 12292
  9.5 52.1 %copy-start.4 = (bf16[32,3,1024]{2,0,1:T(8,128)(2,1)S(1)}, bf16[32,3,1024]{2,0,1:T(8,128)(2,1)}, u32[]{:S(2)}) copy-start(bf16[32,3,1024]{2,0,1:T(8,128)(2,1)} %param.23) | copy-start | bytes 589828
  9.5 52.1 %copy-start.9 = (f32[4,1024]{1,0:T(4,128)S(1)}, f32[4,1024]{1,0:T(4,128)}, u32[]{:S(2)}) copy-start(f32[4,1024]{1,0:T(4,128)} %param.27) | copy-start | bytes 49156
  25.5 36.8 %copy-start.15 = (bf16[16,64,64]{2,1,0:T(8,128)(2,1)S(1)}, bf16[16,64,64]{2,1,0:T(8,128)(2,1)}, u32[]{:S(2)}) copy-start(bf16[16,64,64]{2,1,0:T(8,128)(2,1)} %param.29) | copy-start | bytes 393220
  28.9 34.0 %copy-start.6 = (f32[32,1024]{1,0:T(8,128)S(1)}, f32[32,1024]{1,0:T(8,128)}, u32[]{:S(2)}) copy-start(f32[32,1024]{1,0:T(8,128)} %param.22) | copy-start | bytes 393220
  28.9 113.6 %all-gather.3.cloned.1.call-start = ((), (), s32[]{:S(2)}) async-start(), calls=%async_computation.7 | async-start | bytes 9437184 | tf_op jit(solution)/shard_map/all_gather | solution.py:75
  29.7 160.2 %all-reduce.4.cloned.1.call-start = ((), (), s32[]{:S(2)}) async-start(), calls=%async_computation.8 | async-start | bytes 524288 | tf_op jit(solution)/shard_map/psum | solution.py:80
  60.7 81.8 %copy-start.5 = (bf16[32,2048]{1,0:T(8,128)(2,1)S(1)}, bf16[32,2048]{1,0:T(8,128)(2,1)}, u32[]{:S(2)}) copy-start(bf16[32,2048]{1,0:T(8,128)(2,1)} %reduce-scatter.3.cloned.1.call-done) | copy-start | bytes 393220
  63.0 85.1 %copy-start.3 = (f32[32,1024]{1,0:T(8,128)}, f32[32,1024]{1,0:T(8,128)S(1)}, u32[]{:S(2)}) copy-start(f32[32,1024]{1,0:T(8,128)S(1)} %multiply_add_fusion) | copy-start | bytes 393220
  63.0 126.8 %copy-start.1 = (bf16[32,4096]{1,0:T(8,128)(2,1)S(1)}, bf16[32,4096]{1,0:T(8,128)(2,1)}, u32[]{:S(2)}) copy-start(bf16[32,4096]{1,0:T(8,128)(2,1)} %param.21) | copy-start | bytes 786436
  63.0 128.0 %copy-start.8 = (f32[4096]{0:T(1024)S(1)}, f32[4096]{0:T(1024)}, u32[]{:S(2)}) copy-start(f32[4096]{0:T(1024)} %param.32) | copy-start | bytes 49156
  63.1 143.2 %copy-start.13 = (bf16[512,512]{1,0:T(8,128)(2,1)S(1)}, bf16[512,512]{1,0:T(8,128)(2,1)}, u32[]{:S(2)}) copy-start(bf16[512,512]{1,0:T(8,128)(2,1)} %param.39) | copy-start | bytes 1572868
  63.1 143.2 %copy-start.14 = (bf16[512,512]{1,0:T(8,128)(2,1)S(1)}, bf16[512,512]{1,0:T(8,128)(2,1)}, u32[]{:S(2)}) copy-start(bf16[512,512]{1,0:T(8,128)(2,1)} %param.38) | copy-start | bytes 1572868
  148.2 60.0 %copy-start.10 = (s32[32,2]{0,1:T(2,128)S(1)}, s32[32,2]{0,1:T(2,128)}, u32[]{:S(2)}) copy-start(s32[32,2]{0,1:T(2,128)} %param.34) | copy-start | bytes 772
  148.2 90.2 %reduce-scatter.5.cloned.1.call-start = ((), (), s32[]{:S(2)}) async-start(), calls=%async_computation.9 | async-start | bytes 589824 | tf_op jit(solution)/shard_map/reduce_scatter | solution.py:134
  207.6 81.4 %all-gather.5.cloned.1.call-start = ((), (), s32[]{:S(2)}) async-start(), calls=%async_computation.10 | async-start | bytes 4718592 | tf_op jit(solution)/shard_map/all_gather | solution.py:147
  210.3 82.4 %all-to-all-start.1 = ((bf16[8,16,4096]{2,1,0:T(8,128)(2,1)}), bf16[8,16,4096]{2,1,0:T(8,128)(2,1)S(1)}, u32[]{:S(2)}, u32[]{:S(2)}) async-start(bf16[8,16,4096]{2,1,0:T(8,128)(2,1)} %bitcast.9), calls=%async_computation.2 | async-start | bytes 2097152 | tf_op jit(solution)/shard_map/all_to_all | solution.py:116
  213.9 143.0 %all-reduce.6.cloned.1.call-start = ((), (), s32[]{:S(2)}) async-start(), calls=%async_computation.11 | async-start | bytes 2621440 | tf_op jit(solution)/shard_map/psum | solution.py:123
  295.6 65.9 %copy-start.11 = (bf16[4096]{0:T(1024)(128)(2,1)S(1)}, bf16[4096]{0:T(1024)(128)(2,1)}, u32[]{:S(2)}) copy-start(bf16[4096]{0:T(1024)(128)(2,1)} %param.41) | copy-start | bytes 24580
  295.6 66.6 %copy-start.7 = (bf16[4096,8]{0,1:T(8,128)(2,1)S(1)}, bf16[4096,8]{0,1:T(8,128)(2,1)}, u32[]{:S(2)}) copy-start(bf16[4096,8]{0,1:T(8,128)(2,1)} %param.33) | copy-start | bytes 196612
  301.5 86.5 %copy-start.2 = (bf16[32,4096]{1,0:T(8,128)(2,1)S(1)}, bf16[32,4096]{1,0:T(8,128)(2,1)}, u32[]{:S(2)}) copy-start(bf16[32,4096]{1,0:T(8,128)(2,1)} %all-reduce.4.cloned.1.call-done) | copy-start | bytes 786436
  356.9 31.2 %all-to-all-start.2 = ((bf16[8,16,4096]{2,1,0:T(8,128)(2,1)}), bf16[8,16,4096]{2,1,0:T(8,128)(2,1)S(1)}, u32[]{:S(2)}, u32[]{:S(2)}) async-start(bf16[8,16,4096]{2,1,0:T(8,128)(2,1)} %get-tuple-element.3), calls=%async_computation.3 | async-start | bytes 2097152 | tf_op jit(solution)/shard_map/all_to_all | solution.py:124
Sparse Core Ops, SparseCore 0:
  29.1 31.6 reduce-scatter.2
  62.3 80.1 all-gather.2
  148.3 41.5 all-reduce.3
  207.7 30.6 reduce-scatter.4
  239.8 49.1 all-gather.4
  301.7 55.1 all-reduce.5
where the time goes:
time: 398 us; the launch traced here: 397 us
  waiting for transfers between devices  308 us (77%)
  blocking collectives  30.1 us (8%)
  matrix products  26.9 us (7%)
  between operations  14.4 us (4%)
  starting transfers between devices  8.4 us (2%)
  other arithmetic  6.59 us (2%)
    all_gather x1, waiting for transfers between devices, on_device(): lax.all_gather(out_weight, 'ep', axis=1, tiled=True)  79.5 us
    psum x1, waiting for transfers between devices, on_device(): total = lax.psum(partial_value.astype(jnp.bfloat16), 'tp')  55.4 us
    all_gather x1, waiting for transfers between devices, on_device(): lax.all_gather(dense_down, 'ep', axis=1, tiled=True)  49.8 us
    psum x1, waiting for transfers between devices, on_device(): lax.psum(mixer_part.astype(jnp.bfloat16), 'tp').astype(jnp.float32)  41.6 us
    reduce_scatter x1, waiting for transfers between devices, on_device(): lax.psum_scatter(jnp.dot(arrived, joined, preferred_element_type=jnp.floa...  30.9 us
    all_to_all x1, waiting for transfers between devices, on_device(): lax.all_to_all(total.reshape(sources, items, total.shape[1]), 'ep', split...  25.4 us
    reduce_scatter x1, waiting for transfers between devices, on_device(): lax.psum_scatter(jnp.dot(dense_arrived, dense_joined, preferred_element_t...  24.5 us
    all_to_all x1, blocking collectives, on_device(): lax.all_to_all(normed, 'ep', split_axis=1, concat_axis=0, tiled=True)  16 us
  transfers between devices with their start and end apart: 8, of which 7 were waited for; matrix products, arithmetic and copies ran while one was open for 3% of the time, Pallas kernels for 0%

commit v1 on v0

--- a/solution.py
+++ b/solution.py
@@ -1,3 +1,4 @@
+import functools
 import jax
 import jax.numpy as jnp
 from jax import lax
@@ -6,6 +7,15 @@
 TOP_K = 2
 epsilon = 1e-06
 decay_scale = 8.0
+
+
+def wrap_the_arrays(frame_in, which_axis):
+    big = jnp.stack([frame_in for _ in range(lax.axis_size(which_axis))], axis=0)
+    b_now = lax.all_to_all(big, which_axis, 0, 0)
+    return jnp.concatenate(b_now, 1)
+
+
+_change_strips_all = functools.partial(wrap_the_arrays, which_axis="ep")
 
 
 def rms_scale(rows, gain):
@@ -71,9 +81,7 @@
     ) * input_gate * conv_out.astype(jnp.float32)
     mixer_rows = (new_state * jax.nn.gelu(gate_branch.astype(jnp.float32))).astype(jnp.bfloat16)
     mixer_part = jnp.dot(
-        mixer_rows,
-        lax.all_gather(out_weight, "ep", axis=1, tiled=True),
-        preferred_element_type=jnp.float32,
+        mixer_rows, _change_strips_all(out_weight), preferred_element_type=jnp.float32
     )
     resid = (
         tokens.astype(jnp.float32)

time: 398 us -> 486 us (1.22)
  waiting for transfers between devices: 308 us -> 394 us
  blocking collectives: 30.1 us -> 14.1 us
  starting transfers between devices: 8.4 us -> 19.8 us
  local copies, waits for them, and re-layouts: 2.18 us -> 8.69 us
    all_to_all x0 -> x2, waiting for transfers between devices: none -> 146 us  [the longest x1 138 us: wrap_the_arrays(): b_now = lax.all_to_all(big, which_axis, 0, 0)]
    all_gather x1 -> x0, waiting for transfers between devices: 79.5 us -> none  [on_device(): lax.all_gather(out_weight, 'ep', axis=1, tiled=True)]
    reduce_scatter x1, waiting for transfers between devices: 30.9 us -> 50.9 us  [on_device(): lax.psum_scatter(jnp.dot(arrived, joined, preferred_element_type=jnp.floa...]
    all_to_all x1 -> x0, blocking collectives: 16 us -> none  [on_device(): lax.all_to_all(normed, 'ep', split_axis=1, concat_axis=0, tiled=True)]
    all_to_all x0 -> x2, starting transfers between devices: none -> 11.4 us  [the longest x1 6.35 us: on_device(): lax.all_to_all(normed, 'ep', split_axis=1, concat_axis=0, tiled=True)]
  transfers between devices with their start and end apart: 8 -> 9, of which waited for: 7 -> 8; matrix products, arithmetic and copies ran while one was open for 3% -> 3% of each run, Pallas kernels for 0% -> 0%
where the time goes in v1:
time: 486 us; the launch traced here: 485 us
  waiting for transfers between devices  394 us (81%)
  matrix products  27.3 us (6%)
  starting transfers between devices  19.8 us (4%)
  blocking collectives  14.1 us (3%)
  between operations  14.1 us (3%)
  local copies, waits for them, and re-layouts  8.69 us (2%)
  other arithmetic  6.6 us (1%)
    all_to_all x1, waiting for transfers between devices, wrap_the_arrays(): b_now = lax.all_to_all(big, which_axis, 0, 0)  138 us
    psum x1, waiting for transfers between devices, on_device(): total = lax.psum(partial_value.astype(jnp.bfloat16), 'tp')  55.4 us
    reduce_scatter x1, waiting for transfers between devices, on_device(): lax.psum_scatter(jnp.dot(arrived, joined, preferred_element_type=jnp.floa...  50.9 us
    all_gather x1, waiting for transfers between devices, on_device(): lax.all_gather(dense_down, 'ep', axis=1, tiled=True)  49.7 us
    psum x1, waiting for transfers between devices, on_device(): lax.psum(mixer_part.astype(jnp.bfloat16), 'tp').astype(jnp.float32)  42.1 us
    all_to_all x1, waiting for transfers between devices, on_device(): lax.all_to_all(total.reshape(sources, items, total.shape[1]), 'ep', split...  25.4 us
    reduce_scatter x1, waiting for transfers between devices, on_device(): lax.psum_scatter(jnp.dot(dense_arrived, dense_joined, preferred_element_t...  24.5 us
    all_to_all x1, blocking collectives, on_device(): lax.all_to_all(normed_ffn, 'ep', split_axis=1, concat_axis=0, tiled=True)  14.1 us
  transfers between devices with their start and end apart: 9, of which 8 were waited for; matrix products, arithmetic and copies ran while one was open for 3% of the time, Pallas kernels for 0%

profile of v1, /device:TPU:0, one launch (start us, length us, event | category | flops | bytes accessed | tf_op | source)
XLA Modules:
  0.0 485.0 jit_solution(17756099059100083999)
XLA Ops:
  7.2 1.2 fusion.33
  8.3 1.1 fusion.35
  9.4 0.7 copy.73
  10.2 6.4 %all-to-all-start = ((bf16[32,8,512]{2,0,1:T(8,128)(2,1)}), bf16[32,8,512]{2,0,1:T(8,128)(2,1)S(1)}, u32[]{:S(2)}, u32[]{:S(2)}) async-start(bf16[32,8,512]{2,0,1:T(8,128)(2,1)} %bitcast.73), calls=%async_computation | async-start | bytes 524288 | tf_op jit(solution)/shard_map/all_to_all | solution.py:53
  16.5 1.5 copy.60
  18.0 8.2 %all-to-all-done = bf16[32,8,512]{2,0,1:T(8,128)(2,1)S(1)} async-done(((bf16[32,8,512]{2,0,1:T(8,128)(2,1)}), bf16[32,8,512]{2,0,1:T(8,128)(2,1)S(1)}, u32[]{:S(2)}, u32[]{:S(2)}) %all-to-all-start) | async-done | bytes 262176 | tf_op jit(solution)/shard_map/all_to_all | solution.py:53
  26.2 4.3 stack.2
  30.6 5.1 %all-to-all-start.1 = ((bf16[8,1024,512]{1,2,0:T(8,128)(2,1)}), bf16[8,1024,512]{1,2,0:T(8,128)(2,1)}, u32[]{:S(2)}, u32[]{:S(2)}) async-start(bf16[8,1024,512]{1,2,0:T(8,128)(2,1)} %stack.2), calls=%async_computation.2 | async-start | bytes 16777216 | tf_op jit(solution)/shard_map/all_to_all | solution.py:14
  35.8 1.7 convolution_convert_fusion.4
  37.6 50.9 %reduce-scatter.3.cloned.1.call-done = bf16[32,2048]{1,0:T(8,128)(2,1)} async-done(((bf16[256,2048]{1,0:T(8,128)(2,1)}), bf16[32,2048]{1,0:T(8,128)(2,1)}) %reduce-scatter.3.cloned.1.call-update) | async-done | bytes 131088 | tf_op jit(solution)/shard_map/reduce_scatter | solution.py:55
  88.4 0.9 slice_bitcast_fusion
  90.1 1.2 fusion.17
  91.7 137.7 %all-to-all-done.1 = bf16[8,1024,512]{1,2,0:T(8,128)(2,1)} async-done(((bf16[8,1024,512]{1,2,0:T(8,128)(2,1)}), bf16[8,1024,512]{1,2,0:T(8,128)(2,1)}, u32[]{:S(2)}, u32[]{:S(2)}) %all-to-all-start.1) | async-done | bytes 8388640 | tf_op jit(solution)/shard_map/all_to_all | solution.py:14
  229.4 6.7 %convolution_convert_fusion.3 = bf16[32,4096]{1,0:T(8,128)(2,1)} fusion(bf16[1024,4096]{0,1:T(8,128)(2,1)} %bitcast.6, f32[32,1024]{1,0:T(8,128)S(1)} %multiply_add_fusion, bf16[32,2048]{1,0:T(8,128)(2,1)S(1)} %copy-done.5), kind=kOutput, calls=%fused_computation.6 | convolution fusion | flops 268926976 | bytes 8847360 | tf_op jit(solution)/shard_map/dot_general | solution.py:83
  236.2 42.1 %all-reduce.4.cloned.1.call-done = bf16[32,4096]{1,0:T(8,128)(2,1)} async-done(((bf16[32,4096]{1,0:T(8,128)(2,1)}), bf16[32,4096]{1,0:T(8,128)(2,1)}) %all-reduce.4.cloned.1.call-update) | async-done | bytes 262160 | tf_op jit(solution)/shard_map/psum | solution.py:88
  278.3 1.1 fusion.37
  279.4 1.1 fusion.39
  280.5 14.1 %all_to_all.53 = bf16[32,8,512]{2,0,1:T(8,128)(2,1)S(1)} all-to-all(bf16[32,8,512]{2,0,1:T(8,128)(2,1)S(1)} %bitcast.80), channel_id=1, replica_groups=mesh['ep'=8,'tp'=4] {'ep'}, dimensions={1} | all-to-all | bytes 524288 | tf_op jit(solution)/shard_map/all_to_all | solution.py:140
  294.6 1.3 convolution_convert_fusion.5
  297.3 1.4 convolution_convert_fusion.1
  298.7 3.6 all-to-all-start.2
  302.3 24.5 %reduce-scatter.5.cloned.1.call-done = bf16[32,1024]{1,0:T(8,128)(2,1)} async-done(((bf16[256,1024]{1,0:T(8,128)(2,1)}), bf16[32,1024]{1,0:T(8,128)(2,1)}) %reduce-scatter.5.cloned.1.call-update) | async-done | bytes 65552 | tf_op jit(solution)/shard_map/reduce_scatter | solution.py:142
  326.8 0.8 convert_element_type.109
  327.6 49.7 %all-gather.2.cloned.1.call-done = bf16[512,4096]{1,0:T(8,128)(2,1)} async-done(((bf16[512,512]{1,0:T(8,128)(2,1)}), bf16[512,4096]{1,0:T(8,128)(2,1)}) %all-gather.2.cloned.1.call-update) | async-done | bytes 4194320 | tf_op jit(solution)/shard_map/all_gather | solution.py:155
  377.4 3.7 convolution_convert_fusion.2
  381.1 2.9 fusion.5
  384.0 5.9 %convolution_convert_fusion = bf16[128,4096]{1,0:T(8,128)(2,1)} fusion(bf16[1,512,4096]{2,1,0:T(8,128)(2,1)} %param.37, bf16[128,4096]{1,0:T(8,128)(2,1)S(1)} %bitcast.75, bf16[1,4096,512]{2,1,0:T(8,128)(2,1)} %param.36, f32[128,512]{1,0:T(8,128)S(1)} %fusion.5), kind=kOutput, calls=%fused_computation | convolution fusion | flops 1074659328 | bytes 10747904 | tf_op jit(solution)/shard_map/dot_general | solution.py:130
  389.9 55.4 %all-reduce.6.cloned.1.call-done = (bf16[8,16,4096]{2,1,0:T(8,128)(2,1)}, bf16[32,4096]{1,0:T(8,128)(2,1)}) async-done(((bf16[8,16,4096]{2,1,0:T(8,128)(2,1)}, bf16[32,4096]{1,0:T(8,128)(2,1)}), (bf16[8,16,4096]{2,1,0:T(8,128)(2,1)}, bf16[32,4096]{1,0:T(8,128)(2,1)})) %all-reduce.6.cloned.1.call-update) | async-done | bytes 1310736 | tf_op jit(solution)/shard_map/psum | solution.py:131
  445.3 4.6 all-to-all-start.3
  449.9 0.7 fusion.45
  451.0 25.4 %all-to-all-done.3 = bf16[8,16,4096]{2,1,0:T(8,128)(2,1)S(1)} async-done(((bf16[8,16,4096]{2,1,0:T(8,128)(2,1)}), bf16[8,16,4096]{2,1,0:T(8,128)(2,1)S(1)}, u32[]{:S(2)}, u32[]{:S(2)}) %all-to-all-start.3) | async-done | bytes 1048608 | tf_op jit(solution)/shard_map/all_to_all | solution.py:132
  476.4 2.0 fusion.1
  (73 shorter events, 3.2 us)
Async XLA Ops:
  7.2 82.4 %copy-start = (bf16[16,64,64]{2,1,0:T(8,128)(2,1)S(1)}, bf16[16,64,64]{2,1,0:T(8,128)(2,1)}, u32[]{:S(2)}) copy-start(bf16[16,64,64]{2,1,0:T(8,128)(2,1)} %param.29) | copy-start | bytes 393220
  10.2 16.1 %all-to-all-start = ((bf16[32,8,512]{2,0,1:T(8,128)(2,1)}), bf16[32,8,512]{2,0,1:T(8,128)(2,1)S(1)}, u32[]{:S(2)}, u32[]{:S(2)}) async-start(bf16[32,8,512]{2,0,1:T(8,128)(2,1)} %bitcast.73), calls=%async_computation | async-start | bytes 524288 | tf_op jit(solution)/shard_map/all_to_all | solution.py:53
  30.6 5.2 %copy-start.13 = (bf16[512,1024]{1,0:T(8,128)(2,1)S(1)}, bf16[512,1024]{1,0:T(8,128)(2,1)}, u32[]{:S(2)}) copy-start(bf16[512,1024]{1,0:T(8,128)(2,1)} %param.26) | copy-start | bytes 3145732
  30.6 5.2 %copy-start.14 = (bf16[512,1024]{1,0:T(8,128)(2,1)S(1)}, bf16[512,1024]{1,0:T(8,128)(2,1)}, u32[]{:S(2)}) copy-start(bf16[512,1024]{1,0:T(8,128)(2,1)} %param.25) | copy-start | bytes 3145732
  30.6 198.8 %all-to-all-start.1 = ((bf16[8,1024,512]{1,2,0:T(8,128)(2,1)}), bf16[8,1024,512]{1,2,0:T(8,128)(2,1)}, u32[]{:S(2)}, u32[]{:S(2)}) async-start(bf16[8,1024,512]{1,2,0:T(8,128)(2,1)} %stack.2), calls=%async_computation.2 | async-start | bytes 16777216 | tf_op jit(solution)/shard_map/all_to_all | solution.py:14
  35.6 1.9 copy-start.12
  35.7 53.7 %copy-start.3 = (bf16[32,3,1024]{2,0,1:T(8,128)(2,1)S(1)}, bf16[32,3,1024]{2,0,1:T(8,128)(2,1)}, u32[]{:S(2)}) copy-start(bf16[32,3,1024]{2,0,1:T(8,128)(2,1)} %param.23) | copy-start | bytes 589828
  35.7 53.7 %copy-start.9 = (f32[4,1024]{1,0:T(4,128)S(1)}, f32[4,1024]{1,0:T(4,128)}, u32[]{:S(2)}) copy-start(f32[4,1024]{1,0:T(4,128)} %param.27) | copy-start | bytes 49156
  35.7 52.7 %reduce-scatter.3.cloned.1.call-start = ((), (), s32[]{:S(2)}) async-start(), calls=%async_computation.7 | async-start | bytes 1179648 | tf_op jit(solution)/shard_map/reduce_scatter | solution.py:55
  37.5 54.1 %copy-start.6 = (f32[32,1024]{1,0:T(8,128)S(1)}, f32[32,1024]{1,0:T(8,128)}, u32[]{:S(2)}) copy-start(f32[32,1024]{1,0:T(8,128)} %param.22) | copy-start | bytes 393220
  37.5 240.8 %all-reduce.4.cloned.1.call-start = ((), (), s32[]{:S(2)}) async-start(), calls=%async_computation.8 | async-start | bytes 524288 | tf_op jit(solution)/shard_map/psum | solution.py:88
  88.4 140.9 %copy-start.5 = (bf16[32,2048]{1,0:T(8,128)(2,1)S(1)}, bf16[32,2048]{1,0:T(8,128)(2,1)}, u32[]{:S(2)}) copy-start(bf16[32,2048]{1,0:T(8,128)(2,1)} %reduce-scatter.3.cloned.1.call-done) | copy-start | bytes 393220
  91.7 144.5 %copy-start.4 = (f32[32,1024]{1,0:T(8,128)}, f32[32,1024]{1,0:T(8,128)S(1)}, u32[]{:S(2)}) copy-start(f32[32,1024]{1,0:T(8,128)S(1)} %multiply_add_fusion) | copy-start | bytes 393220
  229.3 48.9 %copy-start.1 = (bf16[32,4096]{1,0:T(8,128)(2,1)S(1)}, bf16[32,4096]{1,0:T(8,128)(2,1)}, u32[]{:S(2)}) copy-start(bf16[32,4096]{1,0:T(8,128)(2,1)} %param.21) | copy-start | bytes 786436
  229.3 50.1 %copy-start.8 = (f32[4096]{0:T(1024)S(1)}, f32[4096]{0:T(1024)}, u32[]{:S(2)}) copy-start(f32[4096]{0:T(1024)} %param.32) | copy-start | bytes 49156
  229.3 65.3 %copy-start.15 = (bf16[512,512]{1,0:T(8,128)(2,1)S(1)}, bf16[512,512]{1,0:T(8,128)(2,1)}, u32[]{:S(2)}) copy-start(bf16[512,512]{1,0:T(8,128)(2,1)} %param.39) | copy-start | bytes 1572868
  229.4 65.3 %copy-start.16 = (bf16[512,512]{1,0:T(8,128)(2,1)S(1)}, bf16[512,512]{1,0:T(8,128)(2,1)}, u32[]{:S(2)}) copy-start(bf16[512,512]{1,0:T(8,128)(2,1)} %param.38) | copy-start | bytes 1572868
  236.1 60.4 %copy-start.10 = (s32[32,2]{0,1:T(2,128)S(1)}, s32[32,2]{0,1:T(2,128)}, u32[]{:S(2)}) copy-start(s32[32,2]{0,1:T(2,128)} %param.34) | copy-start | bytes 772
  236.1 90.6 %reduce-scatter.5.cloned.1.call-start = ((), (), s32[]{:S(2)}) async-start(), calls=%async_computation.9 | async-start | bytes 589824 | tf_op jit(solution)/shard_map/reduce_scatter | solution.py:142
  295.9 81.4 %all-gather.2.cloned.1.call-start = ((), (), s32[]{:S(2)}) async-start(), calls=%async_computation.10 | async-start | bytes 4718592 | tf_op jit(solution)/shard_map/all_gather | solution.py:155
  298.7 82.4 %all-to-all-start.2 = ((bf16[8,16,4096]{2,1,0:T(8,128)(2,1)}), bf16[8,16,4096]{2,1,0:T(8,128)(2,1)S(1)}, u32[]{:S(2)}, u32[]{:S(2)}) async-start(bf16[8,16,4096]{2,1,0:T(8,128)(2,1)} %bitcast.11), calls=%async_computation.3 | async-start | bytes 2097152 | tf_op jit(solution)/shard_map/all_to_all | solution.py:124
  302.3 143.0 %all-reduce.6.cloned.1.call-start = ((), (), s32[]{:S(2)}) async-start(), calls=%async_computation.11 | async-start | bytes 2621440 | tf_op jit(solution)/shard_map/psum | solution.py:131
  384.0 65.9 %copy-start.11 = (bf16[4096]{0:T(1024)(128)(2,1)S(1)}, bf16[4096]{0:T(1024)(128)(2,1)}, u32[]{:S(2)}) copy-start(bf16[4096]{0:T(1024)(128)(2,1)} %param.41) | copy-start | bytes 24580
  384.0 66.6 %copy-start.7 = (bf16[4096,8]{0,1:T(8,128)(2,1)S(1)}, bf16[4096,8]{0,1:T(8,128)(2,1)}, u32[]{:S(2)}) copy-start(bf16[4096,8]{0,1:T(8,128)(2,1)} %param.33) | copy-start | bytes 196612
  389.9 86.6 %copy-start.2 = (bf16[32,4096]{1,0:T(8,128)(2,1)S(1)}, bf16[32,4096]{1,0:T(8,128)(2,1)}, u32[]{:S(2)}) copy-start(bf16[32,4096]{1,0:T(8,128)(2,1)} %all-reduce.4.cloned.1.call-done) | copy-start | bytes 786436
  445.3 31.2 %all-to-all-start.3 = ((bf16[8,16,4096]{2,1,0:T(8,128)(2,1)}), bf16[8,16,4096]{2,1,0:T(8,128)(2,1)S(1)}, u32[]{:S(2)}, u32[]{:S(2)}) async-start(bf16[8,16,4096]{2,1,0:T(8,128)(2,1)} %get-tuple-element.3), calls=%async_computation.4 | async-start | bytes 2097152 | tf_op jit(solution)/shard_map/all_to_all | solution.py:132
Sparse Core Ops, SparseCore 0:
  38.8 49.6 reduce-scatter.2
  236.3 41.9 all-reduce.3
  296.1 30.6 reduce-scatter.4
  328.2 49.0 all-gather.1
  390.0 55.1 all-reduce.5
